TPU v7x, 32 devices: a whole 2x2x4 slice. The times are simulated.
32 devices in a mesh: sp: 8 (over z, x), tp: 4 (over y, core).
Axes of the slice: x: 2, y: 2, z: 4, core: 2. Of those that a mesh axis runs over, the one named last changes fastest.
Arguments:
- layer_input: bfloat16 [8, 4096, 2048], P(None, ('sp', 'tp')), may hold values from -6 to 6
- norm_gain: bfloat16 [2048], replicated, may hold values from 0.099609375 to 1.8984375
- key_weight: bfloat16 [2048, 1024], replicated, may hold values from -0.125 to 0.125
- value_weight: bfloat16 [2048, 1024], replicated, may hold values from -0.125 to 0.125
- new_query: bfloat16 [8, 1024], P('sp', 'tp'), may hold values from -12 to 12
- score_offset: float32 [8], replicated, may hold values from -10 to -3.5
Outputs:
- key_cache: bfloat16 [8, 4096, 1024], P('sp', None, 'tp')
- value_cache: bfloat16 [8, 4096, 1024], P('sp', None, 'tp')
- first_read: float32 [8, 1024], P('sp', 'tp')
All inputs are finite; a program needn't handle non-finite values.
Results may differ from a plain program's by a relative error of at most 0.0082.
Values may be sent and summed in bfloat16 or wider, within the bound.
A program may use at most 128 MiB of HBM per device.

v0:
```python
import jax
import jax.numpy as jnp
from jax import lax
from jax.sharding import PartitionSpec as P

norm_epsilon = 1e-06


def shards(layer_input, norm_gain, key_weight, value_weight, new_query, score_offset):
    seq_count, positions, model_width = layer_input.shape
    groups = lax.axis_size("tp")
    head_count = score_offset.shape[0]
    local_heads = head_count // groups
    head_dim = new_query.shape[1] // local_heads
    columns = local_heads * head_dim
    score_scale = head_dim ** (-0.5)
    wide = layer_input.astype(jnp.float32)
    normed = (
        wide
        * lax.rsqrt(jnp.mean(wide * wide, axis=-1, keepdims=True) + norm_epsilon)
        * norm_gain.astype(jnp.float32)
    ).astype(jnp.bfloat16)
    key_split = key_weight.reshape(model_width, groups, columns)
    value_split = value_weight.reshape(model_width, groups, columns)
    keys = jnp.einsum(
        "spd,dtc->stpc", normed, key_split, preferred_element_type=jnp.float32
    ).astype(jnp.bfloat16)
    values = jnp.einsum(
        "spd,dtc->stpc", normed, value_split, preferred_element_type=jnp.float32
    ).astype(jnp.bfloat16)
    stacked = jnp.stack((keys, values), axis=2)
    direct = stacked.reshape(seq_count * groups, 2, positions, columns)
    received = lax.all_to_all(direct, ("sp", "tp"), split_axis=0, concat_axis=2, tiled=True)
    arrived = received.reshape(2, -1, columns)
    key_cache = arrived[0][None]
    value_cache = arrived[1][None]
    own_keys = arrived[0].reshape(-1, local_heads, head_dim)
    own_values = arrived[1].reshape(-1, local_heads, head_dim)
    own_offsets = lax.dynamic_slice_in_dim(
        score_offset, lax.axis_index("tp") * local_heads, local_heads
    )
    query_own = new_query.reshape(local_heads, head_dim)
    scores = jnp.einsum("hd,phd->hp", query_own, own_keys, preferred_element_type=jnp.float32)
    scores = scores * score_scale + own_offsets[:, None]
    log_rest = jax.nn.log_sigmoid(-scores)
    later = lax.cumsum(log_rest, axis=1, reverse=True) - log_rest
    weights = jnp.exp(jax.nn.log_sigmoid(scores) + later).astype(jnp.bfloat16)
    reading = jnp.einsum("hp,phd->hd", weights, own_values, preferred_element_type=jnp.float32)
    first_read = reading * lax.rsqrt(
        jnp.mean(reading * reading, axis=-1, keepdims=True) + norm_epsilon
    )
    return (key_cache, value_cache, first_read.reshape(1, columns))


def solution(mesh):
    placed = (P(None, ("sp", "tp"), None), P(), P(), P(), P("sp", "tp"), P())
    return jax.shard_map(
        shards,
        mesh=mesh,
        in_specs=placed,
        out_specs=(P("sp", None, "tp"), P("sp", None, "tp"), P("sp", "tp")),
        check_vma=False,
    )
```

profile of v0, /device:TPU:0, one launch (start us, length us, event | category | flops | bytes accessed | tf_op | source)
XLA Modules:
  0.0 139.0 jit_solution(2495934026409444317)
XLA Ops:
  0.6 0.0 copy-start
  0.6 0.0 copy-start.2
  0.7 0.0 copy-start.3
  0.7 3.2 %fusion = f32[8,128]{1,0:T(8,128)S(1)} fusion(bf16[8,128,2048]{2,1,0:T(8,128)(2,1)} %param.6), kind=kLoop, calls=%fused_computation.2 | loop fusion | flops 6290432 | bytes 4198400 | tf_op jit(solution)/shard_map/reduce_sum | solution.py:20
  3.9 0.0 copy-done.3
  3.9 0.2 copy-done.2
  4.1 0.0 copy-start.4
  4.1 7.2 %fusion.17 = bf16[8,128,4,256]{3,1,2,0:T(8,128)(2,1)S(1)} fusion(bf16[256,4,8,256]{3,2,1,0:T(8,128)(2,1)} %bitcast.94, bf16[8,128,2048]{2,1,0:T(8,128)(2,1)S(1)} %copy-done.2, f32[2048]{0:T(1024)S(1)} %convert_element_type.25, f32[8,128]{1,0:T(8,128)S(1)} %add_rsqrt_fusion), kind=kOutput, calls=%fused_computation.18 | convolution fusion | flops 4304404480 | bytes 10498048 | tf_op jit(solution)/shard_map/spd,dtc->stpc/dot_general | solution.py:28
  11.3 0.0 copy-done.4
  11.3 4.8 %fusion.14 = bf16[8,128,4,256]{3,1,2,0:T(8,128)(2,1)S(1)} fusion(bf16[256,4,8,256]{3,2,1,0:T(8,128)(2,1)S(1)} %bitcast.95, bf16[8,128,2048]{2,1,0:T(8,128)(2,1)S(1)} %copy-done.2, f32[2048]{0:T(1024)S(1)} %convert_element_type.25, f32[8,128]{1,0:T(8,128)S(1)} %add_rsqrt_fusion), kind=kOutput, calls=%fused_computation.17 | convolution fusion | flops 4304404480 | bytes 10498048 | tf_op jit(solution)/shard_map/spd,dtc->stpc/dot_general | solution.py:25
  16.2 2.3 %pad_maximum_fusion = bf16[32,2,128,256]{3,2,1,0:T(8,128)(2,1)} fusion(bf16[32,1,128,256]{3,2,1,0:T(8,128)(2,1)S(1)} %bitcast.88, bf16[32,1,128,256]{3,2,1,0:T(8,128)(2,1)S(1)} %bitcast.89), kind=kLoop, calls=%fused_computation.12 | loop fusion | flops 2097152 | bytes 8388608 | tf_op jit(solution)/shard_map/stack | solution.py:31
  18.5 0.0 copy-start.5
  18.5 7.5 %all-to-all-start = ((bf16[32,2,128,256]{3,2,1,0:T(8,128)(2,1)}), bf16[32,2,128,256]{3,2,1,0:T(8,128)(2,1)}, u32[]{:S(2)}, u32[]{:S(2)}) async-start(bf16[32,2,128,256]{3,2,1,0:T(8,128)(2,1)} %pad_maximum_fusion), calls=%async_computation | async-start | bytes 8388608 | tf_op jit(solution)/shard_map/all_to_all | solution.py:33
  26.0 0.0 copy-done.5
  26.0 0.1 dynamic_slice.3
  26.1 94.1 %all-to-all-done = bf16[32,2,128,256]{3,2,1,0:T(8,128)(2,1)} async-done(((bf16[32,2,128,256]{3,2,1,0:T(8,128)(2,1)}), bf16[32,2,128,256]{3,2,1,0:T(8,128)(2,1)}, u32[]{:S(2)}, u32[]{:S(2)}) %all-to-all-start) | async-done | bytes 4194336 | tf_op jit(solution)/shard_map/all_to_all | solution.py:33
  120.2 3.9 %fusion.30 = (bf16[1,1,32,128,256]{4,3,1,2,0:T(8,128)(2,1)S(1)}, bf16[1,1,32,128,256]{4,3,1,2,0:T(8,128)(2,1)}) fusion(bf16[1,2,32,128,256]{4,3,1,2,0:T(8,128)(2,1)} %bitcast.12), kind=kLoop, calls=%fused_computation.40 | loop fusion | bytes 8388608 | tf_op jit(solution)/shard_map/slice | solution.py:36
  124.2 4.3 %reshape_squeeze.6 = bf16[4096,2,128]{2,1,0:T(2,128)(2,1)} reshape(bf16[1,1,32,128,256]{4,3,1,2,0:T(8,128)(2,1)} %get-tuple-element.4) | data formatting | bytes 4194304 | tf_op jit(solution)/shard_map/reshape;squeeze | solution.py:37
  128.5 0.0 copy-done
  128.5 2.2 %fusion.12 = f32[2,1,4096]{2,1,0:T(1,128)S(1)} fusion(bf16[4096,2,128]{2,1,0:T(2,128)(2,1)} %reshape_squeeze.6, bf16[1,256]{1,0:T(2,128)(2,1)S(1)} %copy-done), kind=kOutput, calls=%fused_computation.15 | convolution fusion | flops 2097152 | bytes 2130432 | tf_op jit(solution)/shard_map/hd,phd->hp/dot_general | solution.py:43
  130.7 0.2 fusion.29
  130.9 2.5 %reduce-window.6 = f32[2,32,128]{2,1,0:T(8,128)S(1)} reduce-window(f32[2,32,128]{2,1,0:T(8,128)S(1)} %bitcast.90, f32[]{:T(128)} %constant.9.clone.1), window={size=1x1x128 pad=0_0x0_0x0_127}, to_apply=%region_1.2 | reduce-window | flops 1040384 | bytes 65540 | tf_op jit(solution)/shard_map/reduce-window
  133.4 0.1 slice_reduce_fusion
  133.5 0.3 reduce-window.9
  133.8 0.1 slice.25
  133.8 0.1 add_bitcast_fusion
  133.9 0.3 fusion.27
  134.2 2.1 %reshape_squeeze.7 = bf16[4096,2,128]{2,1,0:T(2,128)(2,1)} reshape(bf16[1,1,32,128,256]{4,3,1,2,0:T(8,128)(2,1)S(1)} %get-tuple-element.3) | data formatting | bytes 4194304 | tf_op jit(solution)/shard_map/reshape;squeeze | solution.py:38
  136.3 0.0 copy-done.1
  136.3 2.0 %fusion.10 = f32[2,1,128]{2,1,0:T(1,128)S(1)} fusion(bf16[4096,2,128]{2,1,0:T(2,128)(2,1)} %reshape_squeeze.7, bf16[2,4096,1]{1,0,2:T(2,128)(2,1)S(1)} %fusion.27), kind=kOutput, calls=%fused_computation.13 | convolution fusion | flops 2097152 | bytes 2114560 | tf_op jit(solution)/shard_map/hp,phd->hd/dot_general | solution.py:48
  138.3 0.1 multiply_reduce_fusion
  138.4 0.6 broadcast_multiply_fusion
  (5 shorter events, 0.0 us)
Async XLA Ops:
  0.6 127.9 %copy-start = (bf16[1,256]{1,0:T(2,128)(2,1)S(1)}, bf16[1,256]{1,0:T(2,128)(2,1)}, u32[]{:S(2)}) copy-start(bf16[1,256]{1,0:T(2,128)(2,1)} %param.10) | copy-start | bytes 1540
  0.6 3.5 %copy-start.2 = (bf16[8,128,2048]{2,1,0:T(8,128)(2,1)S(1)}, bf16[8,128,2048]{2,1,0:T(8,128)(2,1)}, u32[]{:S(2)}) copy-start(bf16[8,128,2048]{2,1,0:T(8,128)(2,1)} %param.6) | copy-start | bytes 12582916
  0.7 3.3 %copy-start.3 = (bf16[2048]{0:T(1024)(128)(2,1)S(1)}, bf16[2048]{0:T(1024)(128)(2,1)}, u32[]{:S(2)}) copy-start(bf16[2048]{0:T(1024)(128)(2,1)} %param.7) | copy-start | bytes 12292
  4.1 7.2 %copy-start.4 = (bf16[2048,1024]{1,0:T(8,128)(2,1)S(1)}, bf16[2048,1024]{1,0:T(8,128)(2,1)}, u32[]{:S(2)}) copy-start(bf16[2048,1024]{1,0:T(8,128)(2,1)} %param.8) | copy-start | bytes 12582916
  18.5 7.5 %copy-start.5 = (f32[8]{0:T(128)S(1)}, f32[8]{0:T(128)}, u32[]{:S(2)}) copy-start(f32[8]{0:T(128)} %param.11) | copy-start | bytes 100
  18.5 101.7 %all-to-all-start = ((bf16[32,2,128,256]{3,2,1,0:T(8,128)(2,1)}), bf16[32,2,128,256]{3,2,1,0:T(8,128)(2,1)}, u32[]{:S(2)}, u32[]{:S(2)}) async-start(bf16[32,2,128,256]{3,2,1,0:T(8,128)(2,1)} %pad_maximum_fusion), calls=%async_computation | async-start | bytes 8388608 | tf_op jit(solution)/shard_map/all_to_all | solution.py:33
  124.2 12.1 %copy-start.1 = (bf16[1,1,32,128,256]{4,3,1,2,0:T(8,128)(2,1)}, bf16[1,1,32,128,256]{4,3,1,2,0:T(8,128)(2,1)S(1)}, u32[]{:S(2)}) copy-start(bf16[1,1,32,128,256]{4,3,1,2,0:T(8,128)(2,1)S(1)} %get-tuple-element.3) | copy-start | bytes 6291460
where the time goes:
time: 139 us
  waiting for transfers between devices  94.1 us (68%)
  matrix products  16.2 us (12%)
  local copies, waits for them, and re-layouts  10.8 us (8%)
  other arithmetic  9.61 us (7%)
  starting transfers between devices  7.46 us (5%)
    all_to_all x1, waiting for transfers between devices, shards(): lax.all_to_all(direct, ('sp', 'tp'), split_axis=0, concat_axis=2, tiled=T...  94.1 us
    all_to_all x1, starting transfers between devices, shards(): lax.all_to_all(direct, ('sp', 'tp'), split_axis=0, concat_axis=2, tiled=T...  7.46 us
    dot_general x1, matrix products, shards(): jnp.einsum('spd,dtc->stpc', normed, value_split, preferred_element_type=j...  7.19 us
    dot_general x1, matrix products, shards(): jnp.einsum('spd,dtc->stpc', normed, key_split, preferred_element_type=jnp...  4.84 us
    another operation x1, local copies, waits for them, and re-layouts, shards(): own_keys = arrived[0].reshape(-1, local_heads, head_dim)  4.32 us
    slice x1, local copies, waits for them, and re-layouts, shards(): value_cache = arrived[1][None]  3.93 us
    reduce_sum x1, other arithmetic, shards(): jnp.mean(wide * wide, axis=-1, keepdims=True) + norm_epsilon  3.23 us
  transfers between devices with their start and end apart: 1, of which 1 were waited for; matrix products, arithmetic and copies ran while one was open for 0% of the time, Pallas kernels for 0%

commit v1 on v0

--- a/solution.py
+++ b/solution.py
@@ -30,7 +30,10 @@
     ).astype(jnp.bfloat16)
     stacked = jnp.stack((keys, values), axis=2)
     direct = stacked.reshape(seq_count * groups, 2, positions, columns)
-    received = lax.all_to_all(direct, ("sp", "tp"), split_axis=0, concat_axis=2, tiled=True)
+    n_dev = lax.axis_size(("sp", "tp"))
+    tiles = jnp.stack(jnp.split(direct, n_dev, axis=0), axis=0)
+    tiles = lax.all_to_all(tiles, ("sp", "tp"), split_axis=0, concat_axis=0)
+    received = jnp.concatenate(tiles, axis=2)
     arrived = received.reshape(2, -1, columns)
     key_cache = arrived[0][None]
     value_cache = arrived[1][None]

time: 139 us -> 158 us (1.14)
  other arithmetic: 9.61 us -> 28.3 us
    unnamed x2 -> x33, other arithmetic: 0.24 us -> 20.6 us
    dot_general x1, matrix products: 4.84 us -> 7.19 us  [shards(): jnp.einsum('spd,dtc->stpc', normed, key_split, preferred_element_type=jnp...]
    dot_general x1, matrix products: 7.19 us -> 4.84 us  [shards(): jnp.einsum('spd,dtc->stpc', normed, value_split, preferred_element_type=j...]
    another operation x3, other arithmetic: 5.09 us -> 3.44 us
where the time goes in v1:
time: 158 us
  waiting for transfers between devices  94.1 us (60%)
  other arithmetic  28.3 us (18%)
  matrix products  16.2 us (10%)
  local copies, waits for them, and re-layouts  10.8 us (7%)
  starting transfers between devices  7.46 us (5%)
    all_to_all x1, waiting for transfers between devices, shards(): tiles = lax.all_to_all(tiles, ('sp', 'tp'), split_axis=0, concat_axis=0)  94.1 us
    unnamed x33, other arithmetic  20.6 us
    all_to_all x1, starting transfers between devices, shards(): tiles = lax.all_to_all(tiles, ('sp', 'tp'), split_axis=0, concat_axis=0)  7.46 us
    dot_general x1, matrix products, shards(): jnp.einsum('spd,dtc->stpc', normed, key_split, preferred_element_type=jnp...  7.19 us
    dot_general x1, matrix products, shards(): jnp.einsum('spd,dtc->stpc', normed, value_split, preferred_element_type=j...  4.84 us
    another operation x1, local copies, waits for them, and re-layouts, shards(): own_keys = arrived[0].reshape(-1, local_heads, head_dim)  4.32 us
    slice x1, local copies, waits for them, and re-layouts, shards(): value_cache = arrived[1][None]  3.93 us
    reduce_sum x1, other arithmetic, shards(): jnp.mean(wide * wide, axis=-1, keepdims=True) + norm_epsilon  3.23 us
  transfers between devices with their start and end apart: 1, of which 1 were waited for; matrix products, arithmetic and copies ran while one was open for 0% of the time, Pallas kernels for 0%

profile of v1, /device:TPU:0, one launch (start us, length us, event | category | flops | bytes accessed | tf_op | source)
XLA Modules:
  0.0 157.8 jit_solution(10638655297935764112)
XLA Ops:
  0.7 3.2 %fusion = f32[8,128]{1,0:T(8,128)S(1)} fusion(bf16[8,128,2048]{2,1,0:T(8,128)(2,1)} %param.6), kind=kLoop, calls=%fused_computation.64 | loop fusion | flops 6290432 | bytes 4198400 | tf_op jit(solution)/shard_map/reduce_sum | solution.py:20
  4.1 7.2 %fusion.14 = bf16[8,128,4,256]{3,1,2,0:T(8,128)(2,1)S(1)} fusion(bf16[256,4,8,256]{3,2,1,0:T(8,128)(2,1)} %bitcast.278, bf16[8,128,2048]{2,1,0:T(8,128)(2,1)S(1)} %copy-done.2, f32[2048]{0:T(1024)S(1)} %convert_element_type.25, f32[8,128]{1,0:T(8,128)S(1)} %add_rsqrt_fusion), kind=kOutput, calls=%fused_computation.78 | convolution fusion | flops 4304404480 | bytes 10498048 | tf_op jit(solution)/shard_map/spd,dtc->stpc/dot_general | solution.py:25
  11.3 4.8 %fusion.17 = bf16[8,128,4,256]{3,1,2,0:T(8,128)(2,1)S(1)} fusion(bf16[256,4,8,256]{3,2,1,0:T(8,128)(2,1)S(1)} %bitcast.279, bf16[8,128,2048]{2,1,0:T(8,128)(2,1)S(1)} %copy-done.2, f32[2048]{0:T(1024)S(1)} %convert_element_type.25, f32[8,128]{1,0:T(8,128)S(1)} %add_rsqrt_fusion), kind=kOutput, calls=%fused_computation.79 | convolution fusion | flops 4304404480 | bytes 10498048 | tf_op jit(solution)/shard_map/spd,dtc->stpc/dot_general | solution.py:28
  17.5 0.7 bitcast_dynamic-update-slice_fusion.28
  18.1 0.7 bitcast_dynamic-update-slice_fusion.27
  18.8 0.7 bitcast_dynamic-update-slice_fusion.26
  19.5 0.7 bitcast_dynamic-update-slice_fusion.25
  20.1 0.7 bitcast_dynamic-update-slice_fusion.24
  20.8 0.7 bitcast_dynamic-update-slice_fusion.23
  22.1 0.7 bitcast_dynamic-update-slice_fusion.21
  22.8 0.7 bitcast_dynamic-update-slice_fusion.20
  23.4 0.7 bitcast_dynamic-update-slice_fusion.19
  24.1 0.7 bitcast_dynamic-update-slice_fusion.18
  24.8 0.7 bitcast_dynamic-update-slice_fusion.17
  25.4 0.7 bitcast_dynamic-update-slice_fusion.16
  26.1 0.7 bitcast_dynamic-update-slice_fusion.15
  27.4 0.7 bitcast_dynamic-update-slice_fusion.13
  28.0 0.7 bitcast_dynamic-update-slice_fusion.12
  28.7 0.7 bitcast_dynamic-update-slice_fusion.11
  30.0 0.7 bitcast_dynamic-update-slice_fusion.9
  31.3 0.7 bitcast_dynamic-update-slice_fusion.7
  32.0 0.7 bitcast_dynamic-update-slice_fusion.6
  35.3 0.7 bitcast_dynamic-update-slice_fusion.1
  36.6 0.7 fusion.52
  37.2 7.5 %all-to-all-start = ((bf16[32,1,2,128,256]{4,3,2,1,0:T(8,128)(2,1)}), bf16[32,1,2,128,256]{4,3,2,1,0:T(8,128)(2,1)}, u32[]{:S(2)}, u32[]{:S(2)}) async-start(bf16[32,1,2,128,256]{4,3,2,1,0:T(8,128)(2,1)} %fusion.52), calls=%async_computation | async-start | bytes 8388608 | tf_op jit(solution)/shard_map/all_to_all | solution.py:35
  44.8 94.1 %all-to-all-done = bf16[32,1,2,128,256]{4,3,2,1,0:T(8,128)(2,1)} async-done(((bf16[32,1,2,128,256]{4,3,2,1,0:T(8,128)(2,1)}), bf16[32,1,2,128,256]{4,3,2,1,0:T(8,128)(2,1)}, u32[]{:S(2)}, u32[]{:S(2)}) %all-to-all-start) | async-done | bytes 4194336 | tf_op jit(solution)/shard_map/all_to_all | solution.py:35
  139.0 3.9 %fusion.63 = (bf16[1,1,32,128,256]{4,3,1,0,2:T(8,128)(2,1)S(1)}, bf16[1,1,32,128,256]{4,3,1,0,2:T(8,128)(2,1)}) fusion(bf16[1,2,32,128,256]{4,3,1,0,2:T(8,128)(2,1)} %bitcast.41), kind=kLoop, calls=%fused_computation.166 | loop fusion | bytes 8388608 | tf_op jit(solution)/shard_map/slice | solution.py:39
  142.9 4.3 %reshape_squeeze.6 = bf16[4096,2,128]{2,1,0:T(2,128)(2,1)} reshape(bf16[1,1,32,128,256]{4,3,1,0,2:T(8,128)(2,1)} %get-tuple-element.4) | data formatting | bytes 4194304 | tf_op jit(solution)/shard_map/reshape;squeeze | solution.py:40
  147.2 2.2 %fusion.12 = f32[2,1,4096]{2,1,0:T(1,128)S(1)} fusion(bf16[4096,2,128]{2,1,0:T(2,128)(2,1)} %reshape_squeeze.6, bf16[1,256]{1,0:T(2,128)(2,1)S(1)} %copy-done), kind=kOutput, calls=%fused_computation.76 | convolution fusion | flops 2097152 | bytes 2130432 | tf_op jit(solution)/shard_map/hd,phd->hp/dot_general | solution.py:46
  149.6 2.5 %reduce-window.6 = f32[2,32,128]{2,1,0:T(8,128)S(1)} reduce-window(f32[2,32,128]{2,1,0:T(8,128)S(1)} %bitcast.274, f32[]{:T(128)} %constant.9.clone.1), window={size=1x1x128 pad=0_0x0_0x0_127}, to_apply=%region_1.2 | reduce-window | flops 1040384 | bytes 65540 | tf_op jit(solution)/shard_map/reduce-window
  152.9 2.1 %reshape_squeeze.7 = bf16[4096,2,128]{2,1,0:T(2,128)(2,1)} reshape(bf16[1,1,32,128,256]{4,3,1,0,2:T(8,128)(2,1)S(1)} %get-tuple-element.3) | data formatting | bytes 4194304 | tf_op jit(solution)/shard_map/reshape;squeeze | solution.py:41
  155.0 2.0 %fusion.10 = f32[2,1,128]{2,1,0:T(1,128)S(1)} fusion(bf16[4096,2,128]{2,1,0:T(2,128)(2,1)} %reshape_squeeze.7, bf16[2,4096,1]{1,0,2:T(2,128)(2,1)S(1)} %fusion.60), kind=kOutput, calls=%fused_computation.74 | convolution fusion | flops 2097152 | bytes 2114560 | tf_op jit(solution)/shard_map/hp,phd->hd/dot_general | solution.py:51
  (36 shorter events, 9.2 us)
Async XLA Ops:
  0.6 146.6 %copy-start = (bf16[1,256]{1,0:T(2,128)(2,1)S(1)}, bf16[1,256]{1,0:T(2,128)(2,1)}, u32[]{:S(2)}) copy-start(bf16[1,256]{1,0:T(2,128)(2,1)} %param.10) | copy-start | bytes 1540
  0.6 3.5 %copy-start.2 = (bf16[8,128,2048]{2,1,0:T(8,128)(2,1)S(1)}, bf16[8,128,2048]{2,1,0:T(8,128)(2,1)}, u32[]{:S(2)}) copy-start(bf16[8,128,2048]{2,1,0:T(8,128)(2,1)} %param.6) | copy-start | bytes 12582916
  0.7 3.3 %copy-start.3 = (bf16[2048]{0:T(1024)(128)(2,1)S(1)}, bf16[2048]{0:T(1024)(128)(2,1)}, u32[]{:S(2)}) copy-start(bf16[2048]{0:T(1024)(128)(2,1)} %param.7) | copy-start | bytes 12292
  4.1 7.2 %copy-start.4 = (bf16[2048,1024]{1,0:T(8,128)(2,1)S(1)}, bf16[2048,1024]{1,0:T(8,128)(2,1)}, u32[]{:S(2)}) copy-start(bf16[2048,1024]{1,0:T(8,128)(2,1)} %param.9) | copy-start | bytes 12582916
  37.2 7.5 %copy-start.5 = (f32[8]{0:T(128)S(1)}, f32[8]{0:T(128)}, u32[]{:S(2)}) copy-start(f32[8]{0:T(128)} %param.11) | copy-start | bytes 100
  37.2 101.7 %all-to-all-start = ((bf16[32,1,2,128,256]{4,3,2,1,0:T(8,128)(2,1)}), bf16[32,1,2,128,256]{4,3,2,1,0:T(8,128)(2,1)}, u32[]{:S(2)}, u32[]{:S(2)}) async-start(bf16[32,1,2,128,256]{4,3,2,1,0:T(8,128)(2,1)} %fusion.52), calls=%async_computation | async-start | bytes 8388608 | tf_op jit(solution)/shard_map/all_to_all | solution.py:35
  142.9 12.1 %copy-start.1 = (bf16[1,1,32,128,256]{4,3,1,0,2:T(8,128)(2,1)}, bf16[1,1,32,128,256]{4,3,1,0,2:T(8,128)(2,1)S(1)}, u32[]{:S(2)}) copy-start(bf16[1,1,32,128,256]{4,3,1,0,2:T(8,128)(2,1)S(1)} %get-tuple-element.3) | copy-start | bytes 6291460
